TPU v7x, 256 devices: a whole 4x4x8 slice. The times are simulated.
256 devices in a mesh: sp: 16 (over y, x), tp: 16 (over z, core).
Axes of the slice: x: 4, y: 4, z: 8, core: 2. Of those that a mesh axis runs over, the one named last changes fastest.
Arguments:
- queries: bfloat16 [6144, 2048], P('sp', 'tp'), may hold values from -6 to 6
- keys: bfloat16 [6144, 2048], P('sp', 'tp'), may hold values from -6 to 6
- values: bfloat16 [6144, 2048], P('sp', 'tp'), may hold values from -6 to 6
- key_bias: bfloat16 [6144, 32], P('sp', 'tp'), may hold values from -16 to 0
- head_gain: float32 [32, 64], P('tp'), may hold values from 0.1 to 1.9
- out_weight: bfloat16 [2048, 2048], P('tp'), may hold values from -0.125 to 0.125
- residual: bfloat16 [6144, 2048], P(('sp', 'tp')), may hold values from -6 to 6
- norm_gain: float32 [2048], replicated, may hold values from 0.1 to 1.9
- gate_proj: bfloat16 [16, 2048, 7168], P('sp', None, 'tp'), may hold values from -0.125 to 0.125
- up_proj: bfloat16 [16, 2048, 7168], P('sp', None, 'tp'), may hold values from -0.125 to 0.125
- down_proj: bfloat16 [16, 7168, 2048], P('sp', 'tp'), may hold values from -0.0625 to 0.0625
- expert_choice: int32 [6144, 2], P(('sp', 'tp')), may hold values from 0 to 15, all different within a row; in each aligned block of 24 rows (0 to 23, 24 to 47, ...) at most 6 rows name the same one
- expert_weights: float32 [6144, 2], P(('sp', 'tp')), may hold values from 0.2 to 1
Outputs:
- layer_out: bfloat16 [6144, 2048], P(('sp', 'tp'))
Inputs may be any that keep to these rules, and one draw needn't show every extreme that they name: `expert_choice`: in each aligned block of 24 rows (the rows of one device), no expert is named more than 6 times; the two experts of a row differ.
All inputs are finite; a program needn't handle non-finite values.
Results may differ from a plain program's by a relative error of at most 0.019.
Values may be sent and summed in bfloat16 or wider, within the bound.
A program may use at most 128 MiB of HBM per device.

v0:
```python
import jax
import jax.numpy as jnp
from jax import lax
from jax.sharding import PartitionSpec as P

epsilon = 1e-06


def in_one_piece(arrays, axis, dim, along):
    ends, at = ([], 0)
    for a in arrays[:-1]:
        at += a.shape[along]
        ends.append(at)
    both = jnp.concatenate(arrays, axis=along)
    return tuple(jnp.split(lax.all_gather(both, axis, axis=dim, tiled=True), ends, axis=along))


def rms_scaled(values_in):
    return values_in * lax.rsqrt(jnp.mean(values_in * values_in, axis=-1, keepdims=True) + epsilon)


def expert_partial(row_block, gate_matrix, up_matrix, down_matrix):
    gate_part = jnp.dot(row_block, gate_matrix, preferred_element_type=jnp.float32)
    up_part = jnp.dot(row_block, up_matrix, preferred_element_type=jnp.float32)
    hidden = (jax.nn.silu(gate_part) * up_part).astype(jnp.bfloat16)
    return jnp.dot(hidden, down_matrix, preferred_element_type=jnp.float32)


def choice_ranks(routes, experts_all):
    flat_routes = routes.reshape(routes.shape[:-2] + (-1,))
    onehot = (flat_routes[..., None] == jnp.arange(experts_all, dtype=jnp.int32)).astype(jnp.int32)
    before = jnp.cumsum(onehot, axis=-2) - onehot
    return jnp.sum(before * onehot, axis=-1).reshape(routes.shape)


def slot_tokens(slot_index, targets, missing):
    flat_slots = slot_index.reshape(-1)
    owners = jnp.arange(flat_slots.shape[0], dtype=jnp.int32) // 2
    matches = flat_slots[None, :] == jnp.arange(targets, dtype=jnp.int32)[:, None]
    owner_found = jnp.sum(jnp.where(matches, owners[None, :], 0), axis=1)
    return jnp.where(jnp.any(matches, axis=1), owner_found, missing)


def on_device(
    queries,
    keys,
    values,
    key_bias,
    head_gain,
    out_weight,
    residual,
    norm_gain,
    gate_proj,
    up_proj,
    down_proj,
    expert_choice,
    expert_weights,
):
    rows_own = queries.shape[0]
    heads_here = head_gain.shape[0]
    head_size = head_gain.shape[1]
    model_width = out_weight.shape[1]
    seq_devices = lax.axis_size("sp")
    head_devices = lax.axis_size("tp")
    own_start = lax.axis_index("sp") * rows_own
    query_pos = own_start + jnp.arange(rows_own, dtype=jnp.int32)
    query_heads = queries.reshape(rows_own, heads_here, head_size)

    def key_block(slot_state, key_rows, value_rows, bias_rows, key_start):
        key_heads = key_rows.reshape(rows_own, heads_here, head_size)
        value_heads = value_rows.reshape(rows_own, heads_here, head_size)
        scores = jnp.einsum(
            "qhd,khd->hqk", query_heads, key_heads, preferred_element_type=jnp.float32
        ) * head_size ** (-0.5)
        scores = scores + bias_rows.astype(jnp.float32).T[:, None, :]
        key_pos = key_start + jnp.arange(rows_own, dtype=jnp.int32)
        earlier = (key_pos[None, :] < query_pos[:, None])[None, :, :]
        log_drops = jnp.where(earlier, jax.nn.log_sigmoid(-scores), 0.0)
        suffix = lax.cumsum(log_drops, axis=2, reverse=True) - log_drops
        within = jnp.where(earlier, jnp.exp(jax.nn.log_sigmoid(scores) + suffix), 0.0).astype(
            jnp.bfloat16
        )
        block_part = jnp.einsum(
            "hqk,khd->qhd", within, value_heads, preferred_element_type=jnp.float32
        )
        block_index = key_start // rows_own
        sums_new = lax.dynamic_update_index_in_dim(
            slot_state[0], block_part.reshape(rows_own, heads_here * head_size), block_index, 0
        )
        totals_new = lax.dynamic_update_index_in_dim(
            slot_state[1], jnp.sum(log_drops, axis=2), block_index, 0
        )
        return (sums_new, totals_new)

    empty_state = (
        jnp.zeros((seq_devices, rows_own, heads_here * head_size), jnp.float32),
        jnp.zeros((seq_devices, heads_here, rows_own), jnp.float32),
    )
    key_piece, value_piece, bias_piece = in_one_piece((keys, values, key_bias), "sp", 0, 1)

    def visit(block_count, state_in):
        offset = block_count * rows_own

        def take_rows(array):
            return lax.dynamic_slice_in_dim(array, offset, rows_own, 0)

        def compute(state_now):
            return key_block(
                state_now,
                take_rows(key_piece),
                take_rows(value_piece),
                take_rows(bias_piece),
                offset,
            )

        def keep(state_now):
            return state_now

        return lax.cond(offset <= own_start, compute, keep, state_in)

    block_sums, totals = lax.fori_loop(0, key_piece.shape[0] // rows_own, visit, empty_state)
    carried = jnp.sum(totals, axis=0, keepdims=True) - jnp.cumsum(totals, axis=0)
    factors = jnp.exp(carried).transpose(0, 2, 1)[..., None]
    mixture = jnp.sum(
        factors * block_sums.reshape(seq_devices, rows_own, heads_here, head_size), axis=0
    )
    attended = (
        (rms_scaled(mixture) * head_gain)
        .astype(jnp.bfloat16)
        .reshape(rows_own, heads_here * head_size)
    )
    row_share = rows_own // head_devices
    merged = lax.all_to_all(attended, "tp", split_axis=0, concat_axis=1, tiled=True)
    projected = jnp.dot(
        merged,
        lax.all_gather(out_weight, "tp", axis=0, tiled=True),
        preferred_element_type=jnp.float32,
    )
    stream = (residual.astype(jnp.float32) + projected).astype(jnp.bfloat16)
    normed = (rms_scaled(stream.astype(jnp.float32)) * norm_gain).astype(jnp.bfloat16)
    local_experts = gate_proj.shape[0]
    experts_all = local_experts * seq_devices
    capacity = 4 * rows_own // (head_devices * experts_all)
    own_slots = expert_choice * capacity + choice_ranks(expert_choice, experts_all)
    wanted = slot_tokens(own_slots, experts_all * capacity, row_share)
    outgoing = jnp.take(normed, wanted, axis=0, mode="fill", fill_value=0)
    arrived = lax.all_to_all(
        outgoing.reshape(seq_devices, local_experts, capacity, model_width),
        "sp",
        split_axis=0,
        concat_axis=0,
        tiled=True,
    )
    row_piece = lax.all_gather(arrived, "tp", axis=0, tiled=True)
    count_rows = row_piece.shape[0]
    partials = jnp.stack(
        [
            expert_partial(
                row_piece[:, 0].reshape(-1, model_width), gate_proj[0], up_proj[0], down_proj[0]
            ).reshape(count_rows, capacity, model_width)
        ],
        axis=1,
    )
    summed = lax.psum_scatter(partials.astype(jnp.bfloat16), "tp", scatter_dimension=0, tiled=True)
    returned = lax.all_to_all(summed, "sp", split_axis=0, concat_axis=0, tiled=True).reshape(
        experts_all * capacity, model_width
    )
    picked = jnp.take(returned, own_slots, axis=0).astype(jnp.float32)
    combined = jnp.sum(expert_weights[:, :, None] * picked, axis=1)
    return (stream.astype(jnp.float32) + combined).astype(jnp.bfloat16)


def solution(mesh):
    placed = (
        P("sp", "tp"),
        P("sp", "tp"),
        P("sp", "tp"),
        P("sp", "tp"),
        P("tp", None),
        P("tp", None),
        P(("sp", "tp"), None),
        P(),
        P("sp", None, "tp"),
        P("sp", None, "tp"),
        P("sp", "tp", None),
        P(("sp", "tp"), None),
        P(("sp", "tp"), None),
    )
    return jax.shard_map(
        on_device, mesh=mesh, in_specs=placed, out_specs=P(("sp", "tp"), None), check_vma=False
    )
```

profile of v0, /device:TPU:2, one launch (start us, length us, event | category | flops | bytes accessed | tf_op | source)
XLA Modules:
  0.0 624.2 jit_solution(17657157115760941867)
XLA Ops:
  6.6 1.1 copy.96
  7.7 1.0 copy.97
  8.7 1.4 pad_maximum_fusion
  10.9 0.8 copy.98
  15.2 55.1 %all-gather.4.cloned.1.call-done = bf16[6144,258]{0,1:T(8,128)(2,1)} async-done(((bf16[384,258]{0,1:T(8,128)(2,1)}), bf16[6144,258]{0,1:T(8,128)(2,1)}) %all-gather.4.cloned.1.call-update) | async-done | bytes 3170320 | tf_op jit(solution)/shard_map/all_gather | solution.py:15
  70.3 1.5 split.14
  71.8 3.9 fusion.30
  75.7 2.1 broadcast_in_dim.84
  78.4 41.8 %while.17 = (s32[]{:T(128)}, f32[16,384,128]{1,2,0:T(8,128)}, f32[16,2,384]{2,1,0:T(2,128)}, s32[]{:T(128)}, bf16[6144,128]{0,1:T(8,128)(2,1)}, /*index=5*/bf16[...) while((s32[]{:T(128)}, f32[16,384,128]{1,2,0:T(8,128)}, ...), condition=%wide.region_6.7_spmd.clone.clone, body=%wide.region_0.6_spmd.clone.clone.sunk | while | flops 122542848 | bytes 19914736 | solution.py:121
  78.4 20.5 %conditional.4 = ((f32[16,384,128]{1,2,0:T(8,128)}, f32[16,2,384]{2,1,0:T(2,128)})) conditional(s32[]{:T(128)} %convert_element_type.76, (f32[16,384,128]{1,2,0:T(8,128)}, f32[16,2,384]{2,1,0:T(2,128)}) %tuple.55, (s32[]{:T(128)}, bf16[6144,128]{0,1:T(8,128)(2,1)}, s32[]{:T(128)}, bf16[6144,128]{0,1:T(8,128)(2,1)}, bf16[384,2,64]{0,2,1:T(8,128)(2,1)}, ...), branch_computations={%region_1.0_spmd, %region_2.5_spmd} | conditional | flops 122542848 | bytes 19912984 | solution.py:119
  78.4 1.6 constant_dynamic-slice_fusion
  80.8 3.6 fusion.13
  84.4 7.0 %fusion.2 = f32[2,384,3,128]{1,2,3,0:T(4,128)S(1)} fusion(f32[2,384,3,128]{1,3,2,0:T(8,128)S(1)} %bitcast.71), kind=kOutput, calls=%fused_computation.5 | output fusion | flops 37453824 | bytes 2359296 | tf_op jit(solution)/shard_map/reduce-window
  92.0 1.3 reduce-window.5
  93.4 0.7 slice.11
  94.5 1.2 copy-done.1
  95.7 1.6 fusion.10
  97.6 0.7 constant_dynamic-update-slice_fusion
  98.9 20.4 %conditional.4 = ((f32[16,384,128]{1,2,0:T(8,128)}, f32[16,2,384]{2,1,0:T(2,128)})) conditional(s32[]{:T(128)} %convert_element_type.76, (f32[16,384,128]{1,2,0:T(8,128)}, f32[16,2,384]{2,1,0:T(2,128)}) %tuple.55, (s32[]{:T(128)}, bf16[6144,128]{0,1:T(8,128)(2,1)}, s32[]{:T(128)}, bf16[6144,128]{0,1:T(8,128)(2,1)}, bf16[384,2,64]{0,2,1:T(8,128)(2,1)}, ...), branch_computations={%region_1.0_spmd, %region_2.5_spmd} | conditional | flops 122542848 | bytes 19912984 | solution.py:119
  98.9 1.6 constant_dynamic-slice_fusion
  101.4 3.6 fusion.13
  105.0 7.0 %fusion.2 = f32[2,384,3,128]{1,2,3,0:T(4,128)S(1)} fusion(f32[2,384,3,128]{1,3,2,0:T(8,128)S(1)} %bitcast.71), kind=kOutput, calls=%fused_computation.5 | output fusion | flops 37453824 | bytes 2359296 | tf_op jit(solution)/shard_map/reduce-window
  112.5 1.3 reduce-window.5
  113.9 0.7 slice.11
  115.0 1.2 copy-done.1
  116.1 1.6 fusion.10
  120.2 0.8 reduce_sum.74
  121.0 0.8 fusion.24
  121.9 2.2 fusion.14
  125.8 7.1 %all-to-all-start = ((bf16[16,24,128]{2,1,0:T(8,128)(2,1)}), bf16[16,24,128]{2,1,0:T(8,128)(2,1)S(1)}, u32[]{:S(2)}, u32[]{:S(2)}) async-start(bf16[16,24,128]{2,1,0:T(8,128)(2,1)} %multiply_convert_fusion.1), calls=%async_computation | async-start | bytes 196608 | tf_op jit(solution)/shard_map/all_to_all | solution.py:133
  133.0 8.2 %all-to-all-done = bf16[16,24,128]{2,1,0:T(8,128)(2,1)S(1)} async-done(((bf16[16,24,128]{2,1,0:T(8,128)(2,1)}), bf16[16,24,128]{2,1,0:T(8,128)(2,1)S(1)}, u32[]{:S(2)}, u32[]{:S(2)}) %all-to-all-start) | async-done | bytes 98336 | tf_op jit(solution)/shard_map/all_to_all | solution.py:133
  141.3 4.7 multiply_reduce_fusion.1
  146.7 1.0 gather_fusion
  148.0 300.1 %all_to_all.26 = bf16[16,1,6,2048]{3,2,1,0:T(8,128)(2,1)S(1)} all-to-all(bf16[16,1,6,2048]{3,2,1,0:T(8,128)(2,1)S(1)} %select_bitcast_fusion), channel_id=1, replica_groups=mesh['sp'=16,'tp'=16] {'sp'}, dimensions={0} | all-to-all | bytes 786432 | tf_op jit(solution)/shard_map/all_to_all | solution.py:147
  448.0 1.0 copy.108
  449.1 39.8 %all-gather.8.cloned.1.call-done = bf16[256,1,6,2048]{3,0,2,1:T(8,128)(2,1)} async-done(((bf16[16,1,6,2048]{3,0,2,1:T(8,128)(2,1)}), bf16[256,1,6,2048]{3,0,2,1:T(8,128)(2,1)}) %all-gather.8.cloned.1.call-update) | async-done | bytes 6291472 | tf_op jit(solution)/shard_map/all_gather | solution.py:154
  488.9 9.6 %copy.109 = bf16[256,1,6,2048]{3,2,0,1:T(8,128)(2,1)} copy(bf16[256,1,6,2048]{3,0,2,1:T(8,128)(2,1)} %all-gather.8.cloned.1.call-done) | data formatting | bytes 12582912 | tf_op jit(solution)/shard_map/all_gather | solution.py:154
  498.5 11.1 %reshape_squeeze.3 = bf16[1536,2048]{1,0:T(8,128)(2,1)} reshape(bf16[256,1,6,2048]{3,2,0,1:T(8,128)(2,1)} %copy.109) | data formatting | bytes 12582912 | tf_op jit(solution)/shard_map/reshape;squeeze | solution.py:159
  509.6 5.9 fusion.20
  515.5 4.3 fusion.15
  519.8 1.7 copy.110
  521.5 1.7 dot_general.23
  523.2 7.5 %convert_bitcast_fusion.1 = bf16[256,1,6,2048]{3,0,2,1:T(8,128)(2,1)} fusion(bf16[1,448,2048]{2,1,0:T(8,128)(2,1)S(1)} %copy-done, bf16[256,6,448]{2,1,0:T(8,128)(2,1)} %dot_general.23), kind=kOutput, calls=%fused_computation.29 | convolution fusion | flops 2821718016 | bytes 9502720 | tf_op jit(solution)/shard_map/dot_general | solution.py:26
  530.7 65.8 %reduce-scatter.2.cloned.1.call-done = bf16[16,1,6,2048]{3,0,2,1:T(8,128)(2,1)} async-done(((bf16[256,1,6,2048]{3,0,2,1:T(8,128)(2,1)}), bf16[16,1,6,2048]{3,0,2,1:T(8,128)(2,1)}) %reduce-scatter.2.cloned.1.call-update) | async-done | bytes 393232 | tf_op jit(solution)/shard_map/reduce_scatter | solution.py:164
  596.6 2.0 copy.112
  598.6 7.3 %all-to-all-start.2 = ((bf16[16,1,6,2048]{3,2,1,0:T(8,128)(2,1)}), bf16[16,1,6,2048]{3,2,1,0:T(8,128)(2,1)S(1)}, u32[]{:S(2)}, u32[]{:S(2)}) async-start(bf16[16,1,6,2048]{3,2,1,0:T(8,128)(2,1)} %copy.112), calls=%async_computation.3 | async-start | bytes 1048576 | tf_op jit(solution)/shard_map/all_to_all | solution.py:165
  606.3 8.4 %all-to-all-done.2 = bf16[16,1,6,2048]{3,2,1,0:T(8,128)(2,1)S(1)} async-done(((bf16[16,1,6,2048]{3,2,1,0:T(8,128)(2,1)}), bf16[16,1,6,2048]{3,2,1,0:T(8,128)(2,1)S(1)}, u32[]{:S(2)}, u32[]{:S(2)}) %all-to-all-start.2) | async-done | bytes 393248 | tf_op jit(solution)/shard_map/all_to_all | solution.py:165
  615.6 1.4 multiply_reduce_fusion
  (138 shorter events, 15.9 us)
Async XLA Ops:
  6.5 516.7 %copy-start = (bf16[1,448,2048]{2,1,0:T(8,128)(2,1)S(1)}, bf16[1,448,2048]{2,1,0:T(8,128)(2,1)}, u32[]{:S(2)}) copy-start(bf16[1,448,2048]{2,1,0:T(8,128)(2,1)} %param.27) | copy-start | bytes 5505028
  6.5 4.4 copy-start.7
  6.5 5.1 copy-start.18
  6.5 5.7 copy-start.13
  6.5 63.7 %all-gather.4.cloned.1.call-start = ((), (), s32[]{:S(2)}) async-start(), calls=%async_computation.4 | async-start | bytes 3446784 | tf_op jit(solution)/shard_map/all_gather | solution.py:15
  10.1 131.1 %all-gather.6.cloned.1.call-start = ((), (), s32[]{:S(2)}) async-start(), calls=%async_computation.5 | async-start | bytes 8912896 | tf_op jit(solution)/shard_map/all_gather | solution.py:136
  13.5 62.2 %copy-start.10 = (s32[24,2]{0,1:T(2,128)}, s32[24,2]{0,1:T(2,128)S(1)}, u32[]{:S(2)}) copy-start(s32[24,2]{0,1:T(2,128)S(1)} %get-tuple-element.261) | copy-start | bytes 580
  94.3 1.3 copy-start.1
  94.4 2.9 copy-start.2
  95.7 2.6 copy-start.8
  114.9 1.3 copy-start.1
  115.0 2.8 copy-start.2
  116.1 2.6 copy-start.8
  124.1 1.1 copy-start.16
  124.1 8.9 %copy-start.9 = (s32[16,6]{1,0:T(8,128)S(1)}, s32[16,6]{1,0:T(8,128)}, u32[]{:S(2)}) copy-start(s32[16,6]{1,0:T(8,128)} %select_n.105) | copy-start | bytes 1156
  124.1 17.2 %copy-start.6 = (bf16[24,2048]{1,0:T(8,128)(2,1)S(1)}, bf16[24,2048]{1,0:T(8,128)(2,1)}, u32[]{:S(2)}) copy-start(bf16[24,2048]{1,0:T(8,128)(2,1)} %param.23) | copy-start | bytes 294916
  125.8 15.4 %all-to-all-start = ((bf16[16,24,128]{2,1,0:T(8,128)(2,1)}), bf16[16,24,128]{2,1,0:T(8,128)(2,1)S(1)}, u32[]{:S(2)}, u32[]{:S(2)}) async-start(bf16[16,24,128]{2,1,0:T(8,128)(2,1)} %multiply_convert_fusion.1), calls=%async_computation | async-start | bytes 196608 | tf_op jit(solution)/shard_map/all_to_all | solution.py:133
  132.9 356.0 %all-gather.8.cloned.1.call-start = ((), (), s32[]{:S(2)}) async-start(), calls=%async_computation.6 | async-start | bytes 6684672 | tf_op jit(solution)/shard_map/all_gather | solution.py:154
  133.0 13.6 %copy-start.12 = (f32[2048]{0:T(1024)S(1)}, f32[2048]{0:T(1024)}, u32[]{:S(2)}) copy-start(f32[2048]{0:T(1024)} %param.24) | copy-start | bytes 24580
  146.0 0.7 copy-start.4
  449.0 147.6 %reduce-scatter.2.cloned.1.call-start = ((), (), s32[]{:S(2)}) async-start(), calls=%async_computation.7 | async-start | bytes 6684672 | tf_op jit(solution)/shard_map/reduce_scatter | solution.py:164
  509.6 5.9 copy-start.3
  509.6 5.9 copy-start.17
  530.7 75.2 %copy-start.11 = (s32[24,2]{0,1:T(2,128)S(1)}, s32[24,2]{0,1:T(2,128)}, u32[]{:S(2)}) copy-start(s32[24,2]{0,1:T(2,128)} %copy-done.10) | copy-start | bytes 580
  530.7 75.4 %copy-start.14 = (pred[24,2]{0,1:T(4,128)(4,1)S(1)}, pred[24,2]{0,1:T(4,128)(4,1)}, u32[]{:S(2)}) copy-start(pred[24,2]{0,1:T(4,128)(4,1)} %get-tuple-element.260) | copy-start | bytes 148
  530.7 75.5 %copy-start.15 = (f32[24,2]{0,1:T(2,128)S(1)}, f32[24,2]{0,1:T(2,128)}, u32[]{:S(2)}) copy-start(f32[24,2]{0,1:T(2,128)} %param.29) | copy-start | bytes 580
  598.6 16.0 %all-to-all-start.2 = ((bf16[16,1,6,2048]{3,2,1,0:T(8,128)(2,1)}), bf16[16,1,6,2048]{3,2,1,0:T(8,128)(2,1)S(1)}, u32[]{:S(2)}, u32[]{:S(2)}) async-start(bf16[16,1,6,2048]{3,2,1,0:T(8,128)(2,1)} %copy.112), calls=%async_computation.3 | async-start | bytes 1048576 | tf_op jit(solution)/shard_map/all_to_all | solution.py:165
  606.3 10.8 %copy-start.5 = (f32[24,2048]{1,0:T(8,128)S(1)}, f32[24,2048]{1,0:T(8,128)}, u32[]{:S(2)}) copy-start(f32[24,2048]{1,0:T(8,128)} %copy-done.4) | copy-start | bytes 589828
Sparse Core Ops, SparseCore 0:
  10.3 59.9 all-gather.3
  72.1 55.5 all-gather.5
  449.2 39.7 all-gather.7
  530.8 65.7 reduce-scatter.1
where the time goes:
time: 629 us; the launch traced here: 624 us
  blocking collectives  300 us (48%)
  waiting for transfers between devices  178 us (28%)
  local copies, waits for them, and re-layouts  55 us (9%)
  other arithmetic  32.1 us (5%)
  matrix products  30 us (5%)
  starting transfers between devices  14.5 us (2%)
  between operations  13.5 us (2%)
    all_to_all x1, blocking collectives, on_device(): lax.all_to_all(outgoing.reshape(seq_devices, local_experts, capacity, mod...  300 us
    reduce_scatter x1, waiting for transfers between devices, on_device(): lax.psum_scatter(partials.astype(jnp.bfloat16), 'tp', scatter_dimension=0...  65.8 us
    all_gather x1, waiting for transfers between devices, in_one_piece(): lax.all_gather(both, axis, axis=dim, tiled=True)  55.1 us
    all_gather x1, waiting for transfers between devices, on_device(): row_piece = lax.all_gather(arrived, 'tp', axis=0, tiled=True)  39.8 us
    another operation x4, other arithmetic  16.6 us
  transfers between devices with their start and end apart: 6, of which 5 were waited for; matrix products, arithmetic and copies ran while one was open for 9% of the time, Pallas kernels for 0%

commit v1 on v0

--- a/solution.py
+++ b/solution.py
@@ -4,6 +4,11 @@
 from jax.sharding import PartitionSpec as P
 
 epsilon = 1e-06
+
+
+def change_cube(my_data):
+    odd = jnp.stack([my_data for _ in range(lax.psum(1, "tp"))])
+    return jnp.concatenate(lax.all_to_all(odd, "tp", 0, 0), axis=0)
 
 
 def in_one_piece(arrays, axis, dim, along):
@@ -151,7 +156,7 @@
         concat_axis=0,
         tiled=True,
     )
-    row_piece = lax.all_gather(arrived, "tp", axis=0, tiled=True)
+    row_piece = change_cube(arrived)
     count_rows = row_piece.shape[0]
     partials = jnp.stack(
         [

time: 629 us -> 726 us (1.15)
  blocking collectives: 300 us -> 442 us
  waiting for transfers between devices: 178 us -> 135 us
    all_to_all x0 -> x1, blocking collectives: none -> 142 us  [change_cube(): return jnp.concatenate(lax.all_to_all(odd, 'tp', 0, 0), axis=0)]
    all_gather x1 -> x0, waiting for transfers between devices: 39.8 us -> none  [on_device(): row_piece = lax.all_gather(arrived, 'tp', axis=0, tiled=True)]
    all_gather x1 -> x0, local copies, waits for them, and re-layouts: 9.6 us -> none  [on_device(): row_piece = lax.all_gather(arrived, 'tp', axis=0, tiled=True)]
    all_to_all x0 -> x1, local copies, waits for them, and re-layouts: none -> 7.62 us  [change_cube(): return jnp.concatenate(lax.all_to_all(odd, 'tp', 0, 0), axis=0)]
  transfers between devices with their start and end apart: 6 -> 5, of which waited for: 5 -> 4; matrix products, arithmetic and copies ran while one was open for 9% -> 8% of each run, Pallas kernels for 0% -> 0%
where the time goes in v1:
time: 726 us; the launch traced here: 722 us
  blocking collectives  442 us (61%)
  waiting for transfers between devices  135 us (19%)
  local copies, waits for them, and re-layouts  53.1 us (7%)
  other arithmetic  32.1 us (4%)
  matrix products  30.1 us (4%)
  starting transfers between devices  14.5 us (2%)
  between operations  13.4 us (2%)
    all_to_all x1, blocking collectives, on_device(): lax.all_to_all(outgoing.reshape(seq_devices, local_experts, capacity, mod...  300 us
    all_to_all x1, blocking collectives, change_cube(): return jnp.concatenate(lax.all_to_all(odd, 'tp', 0, 0), axis=0)  142 us
    reduce_scatter x1, waiting for transfers between devices, on_device(): lax.psum_scatter(partials.astype(jnp.bfloat16), 'tp', scatter_dimension=0...  62.8 us
    all_gather x1, waiting for transfers between devices, in_one_piece(): lax.all_gather(both, axis, axis=dim, tiled=True)  55 us
    another operation x4, other arithmetic  16.7 us
  transfers between devices with their start and end apart: 5, of which 4 were waited for; matrix products, arithmetic and copies ran while one was open for 8% of the time, Pallas kernels for 0%

profile of v1, /device:TPU:2, one launch (start us, length us, event | category | flops | bytes accessed | tf_op | source)
XLA Modules:
  0.0 721.9 jit_solution(3250621641956478856)
XLA Ops:
  6.6 1.1 copy.96
  7.7 1.0 copy.97
  8.7 1.4 pad_maximum_fusion
  10.9 0.8 copy.98
  15.2 55.0 %all-gather.3.cloned.1.call-done = bf16[6144,258]{0,1:T(8,128)(2,1)} async-done(((bf16[384,258]{0,1:T(8,128)(2,1)}), bf16[6144,258]{0,1:T(8,128)(2,1)}) %all-gather.3.cloned.1.call-update) | async-done | bytes 3170320 | tf_op jit(solution)/shard_map/all_gather | solution.py:20
  70.3 1.5 split.14
  71.8 3.9 fusion.30
  75.7 2.1 broadcast_in_dim.84
  78.4 41.8 %while.17 = (s32[]{:T(128)}, f32[16,384,128]{1,2,0:T(8,128)}, f32[16,2,384]{2,1,0:T(2,128)}, s32[]{:T(128)}, bf16[6144,128]{0,1:T(8,128)(2,1)}, /*index=5*/bf16[...) while((s32[]{:T(128)}, f32[16,384,128]{1,2,0:T(8,128)}, ...), condition=%wide.region_6.7_spmd.clone.clone, body=%wide.region_0.6_spmd.clone.clone.sunk | while | flops 122542848 | bytes 19914736 | solution.py:126
  78.4 20.5 %conditional.4 = ((f32[16,384,128]{1,2,0:T(8,128)}, f32[16,2,384]{2,1,0:T(2,128)})) conditional(s32[]{:T(128)} %convert_element_type.76, (f32[16,384,128]{1,2,0:T(8,128)}, f32[16,2,384]{2,1,0:T(2,128)}) %tuple.55, (s32[]{:T(128)}, bf16[6144,128]{0,1:T(8,128)(2,1)}, s32[]{:T(128)}, bf16[6144,128]{0,1:T(8,128)(2,1)}, bf16[384,2,64]{0,2,1:T(8,128)(2,1)}, ...), branch_computations={%region_1.0_spmd, %region_2.5_spmd} | conditional | flops 122542848 | bytes 19912984 | solution.py:124
  78.4 1.6 constant_dynamic-slice_fusion
  80.9 3.6 fusion.13
  84.5 7.0 fusion.2
  92.1 1.3 reduce-window.5
  93.4 0.7 slice.11
  94.5 1.2 copy-done.1
  95.7 1.6 fusion.10
  98.9 20.4 %conditional.4 = ((f32[16,384,128]{1,2,0:T(8,128)}, f32[16,2,384]{2,1,0:T(2,128)})) conditional(s32[]{:T(128)} %convert_element_type.76, (f32[16,384,128]{1,2,0:T(8,128)}, f32[16,2,384]{2,1,0:T(2,128)}) %tuple.55, (s32[]{:T(128)}, bf16[6144,128]{0,1:T(8,128)(2,1)}, s32[]{:T(128)}, bf16[6144,128]{0,1:T(8,128)(2,1)}, bf16[384,2,64]{0,2,1:T(8,128)(2,1)}, ...), branch_computations={%region_1.0_spmd, %region_2.5_spmd} | conditional | flops 122542848 | bytes 19912984 | solution.py:124
  98.9 1.6 constant_dynamic-slice_fusion
  101.4 3.6 fusion.13
  105.0 7.0 fusion.2
  112.6 1.3 reduce-window.5
  113.9 0.7 slice.11
  115.0 1.2 copy-done.1
  116.1 1.6 fusion.10
  118.1 0.7 constant_dynamic-update-slice_fusion
  120.2 0.8 reduce_sum.74
  121.0 0.8 fusion.24
  121.9 2.2 fusion.14
  125.8 7.1 all-to-all-start
  133.1 8.2 %all-to-all-done = bf16[16,24,128]{2,1,0:T(8,128)(2,1)S(1)} async-done(((bf16[16,24,128]{2,1,0:T(8,128)(2,1)}), bf16[16,24,128]{2,1,0:T(8,128)(2,1)S(1)}, u32[]{:S(2)}, u32[]{:S(2)}) %all-to-all-start) | async-done | bytes 98336 | tf_op jit(solution)/shard_map/all_to_all | solution.py:138
  141.3 4.7 multiply_reduce_fusion.1
  146.8 1.0 gather_fusion
  148.0 300.3 %all_to_all.34 = bf16[16,1,6,2048]{3,2,1,0:T(8,128)(2,1)S(1)} all-to-all(bf16[16,1,6,2048]{3,2,1,0:T(8,128)(2,1)S(1)} %select_bitcast_fusion), channel_id=1, replica_groups=mesh['sp'=16,'tp'=16] {'sp'}, dimensions={0} | all-to-all | bytes 786432 | tf_op jit(solution)/shard_map/all_to_all | solution.py:152
  448.5 0.8 stack.2
  449.3 142.2 %all_to_all.35 = bf16[16,16,1,6,2048]{4,1,3,2,0:T(8,128)(2,1)S(1)} all-to-all(bf16[16,16,1,6,2048]{4,1,3,2,0:T(8,128)(2,1)S(1)} %stack.2), channel_id=1, replica_groups=mesh['sp'=16,'tp'=16] {'tp'}, dimensions={0} | all-to-all | bytes 12582912 | tf_op jit(solution)/shard_map/all_to_all | solution.py:11
  591.5 7.6 %copy.109 = bf16[16,16,1,6,2048]{4,3,1,0,2:T(8,128)(2,1)} copy(bf16[16,16,1,6,2048]{4,1,3,2,0:T(8,128)(2,1)S(1)} %all_to_all.35) | data formatting | bytes 12582912 | tf_op jit(solution)/shard_map/all_to_all | solution.py:11
  599.1 11.0 %reshape_squeeze_reshape.3 = bf16[1536,2048]{1,0:T(8,128)(2,1)} reshape(bf16[16,16,1,6,2048]{4,3,1,0,2:T(8,128)(2,1)} %copy.109) | data formatting | bytes 12582912 | tf_op jit(solution)/shard_map/reshape;squeeze;reshape | solution.py:164
  610.2 6.0 fusion.20
  616.2 4.3 fusion.15
  620.5 1.7 copy.110
  622.2 1.7 dot_general.23
  623.9 7.5 %convert_bitcast_fusion.1 = bf16[256,1,6,2048]{3,0,2,1:T(8,128)(2,1)} fusion(bf16[1,448,2048]{2,1,0:T(8,128)(2,1)S(1)} %copy-done, bf16[256,6,448]{2,1,0:T(8,128)(2,1)} %dot_general.23), kind=kOutput, calls=%fused_computation.29 | convolution fusion | flops 2821718016 | bytes 9502720 | tf_op jit(solution)/shard_map/dot_general | solution.py:31
  631.4 62.8 %reduce-scatter.2.cloned.1.call-done = bf16[16,1,6,2048]{3,0,2,1:T(8,128)(2,1)} async-done(((bf16[256,1,6,2048]{3,0,2,1:T(8,128)(2,1)}), bf16[16,1,6,2048]{3,0,2,1:T(8,128)(2,1)}) %reduce-scatter.2.cloned.1.call-update) | async-done | bytes 393232 | tf_op jit(solution)/shard_map/reduce_scatter | solution.py:169
  694.2 2.0 copy.112
  696.2 7.3 %all-to-all-start.3 = ((bf16[16,1,6,2048]{3,2,1,0:T(8,128)(2,1)}), bf16[16,1,6,2048]{3,2,1,0:T(8,128)(2,1)S(1)}, u32[]{:S(2)}, u32[]{:S(2)}) async-start(bf16[16,1,6,2048]{3,2,1,0:T(8,128)(2,1)} %copy.112), calls=%async_computation.4 | async-start | bytes 1048576 | tf_op jit(solution)/shard_map/all_to_all | solution.py:170
  703.9 8.4 %all-to-all-done.3 = bf16[16,1,6,2048]{3,2,1,0:T(8,128)(2,1)S(1)} async-done(((bf16[16,1,6,2048]{3,2,1,0:T(8,128)(2,1)}), bf16[16,1,6,2048]{3,2,1,0:T(8,128)(2,1)S(1)}, u32[]{:S(2)}, u32[]{:S(2)}) %all-to-all-start.3) | async-done | bytes 393248 | tf_op jit(solution)/shard_map/all_to_all | solution.py:170
  713.2 1.4 multiply_reduce_fusion
  (137 shorter events, 16.1 us)
Async XLA Ops:
  6.5 617.3 %copy-start = (bf16[1,448,2048]{2,1,0:T(8,128)(2,1)S(1)}, bf16[1,448,2048]{2,1,0:T(8,128)(2,1)}, u32[]{:S(2)}) copy-start(bf16[1,448,2048]{2,1,0:T(8,128)(2,1)} %param.27) | copy-start | bytes 5505028
  6.5 4.4 copy-start.7
  6.5 5.1 copy-start.18
  6.5 5.8 copy-start.13
  6.5 63.7 %all-gather.3.cloned.1.call-start = ((), (), s32[]{:S(2)}) async-start(), calls=%async_computation.5 | async-start | bytes 3446784 | tf_op jit(solution)/shard_map/all_gather | solution.py:20
  10.1 131.1 %all-gather.5.cloned.1.call-start = ((), (), s32[]{:S(2)}) async-start(), calls=%async_computation.6 | async-start | bytes 8912896 | tf_op jit(solution)/shard_map/all_gather | solution.py:141
  13.6 62.2 %copy-start.10 = (s32[24,2]{0,1:T(2,128)}, s32[24,2]{0,1:T(2,128)S(1)}, u32[]{:S(2)}) copy-start(s32[24,2]{0,1:T(2,128)S(1)} %get-tuple-element.261) | copy-start | bytes 580
  94.4 1.3 copy-start.1
  94.5 2.9 copy-start.2
  95.7 2.6 copy-start.8
  114.9 1.3 copy-start.1
  115.0 2.8 copy-start.2
  116.1 2.6 copy-start.8
  124.1 1.1 copy-start.16
  124.1 8.9 %copy-start.9 = (s32[16,6]{1,0:T(8,128)S(1)}, s32[16,6]{1,0:T(8,128)}, u32[]{:S(2)}) copy-start(s32[16,6]{1,0:T(8,128)} %select_n.105) | copy-start | bytes 1156
  124.1 17.2 %copy-start.6 = (bf16[24,2048]{1,0:T(8,128)(2,1)S(1)}, bf16[24,2048]{1,0:T(8,128)(2,1)}, u32[]{:S(2)}) copy-start(bf16[24,2048]{1,0:T(8,128)(2,1)} %param.23) | copy-start | bytes 294916
  125.8 15.4 %all-to-all-start = ((bf16[16,24,128]{2,1,0:T(8,128)(2,1)}), bf16[16,24,128]{2,1,0:T(8,128)(2,1)S(1)}, u32[]{:S(2)}, u32[]{:S(2)}) async-start(bf16[16,24,128]{2,1,0:T(8,128)(2,1)} %multiply_convert_fusion.1), calls=%async_computation | async-start | bytes 196608 | tf_op jit(solution)/shard_map/all_to_all | solution.py:138
  133.0 561.2 %reduce-scatter.2.cloned.1.call-start = ((), (), s32[]{:S(2)}) async-start(), calls=%async_computation.7 | async-start | bytes 6684672 | tf_op jit(solution)/shard_map/reduce_scatter | solution.py:169
  133.0 13.6 %copy-start.12 = (f32[2048]{0:T(1024)S(1)}, f32[2048]{0:T(1024)}, u32[]{:S(2)}) copy-start(f32[2048]{0:T(1024)} %param.24) | copy-start | bytes 24580
  146.0 0.7 copy-start.4
  610.2 6.0 copy-start.3
  610.2 6.0 copy-start.17
  631.4 72.1 %copy-start.11 = (s32[24,2]{0,1:T(2,128)S(1)}, s32[24,2]{0,1:T(2,128)}, u32[]{:S(2)}) copy-start(s32[24,2]{0,1:T(2,128)} %copy-done.10) | copy-start | bytes 580
  631.4 72.3 %copy-start.14 = (pred[24,2]{0,1:T(4,128)(4,1)S(1)}, pred[24,2]{0,1:T(4,128)(4,1)}, u32[]{:S(2)}) copy-start(pred[24,2]{0,1:T(4,128)(4,1)} %get-tuple-element.260) | copy-start | bytes 148
  631.4 72.4 %copy-start.15 = (f32[24,2]{0,1:T(2,128)S(1)}, f32[24,2]{0,1:T(2,128)}, u32[]{:S(2)}) copy-start(f32[24,2]{0,1:T(2,128)} %param.29) | copy-start | bytes 580
  696.2 16.1 %all-to-all-start.3 = ((bf16[16,1,6,2048]{3,2,1,0:T(8,128)(2,1)}), bf16[16,1,6,2048]{3,2,1,0:T(8,128)(2,1)S(1)}, u32[]{:S(2)}, u32[]{:S(2)}) async-start(bf16[16,1,6,2048]{3,2,1,0:T(8,128)(2,1)} %copy.112), calls=%async_computation.4 | async-start | bytes 1048576 | tf_op jit(solution)/shard_map/all_to_all | solution.py:170
  703.9 10.8 %copy-start.5 = (f32[24,2048]{1,0:T(8,128)S(1)}, f32[24,2048]{1,0:T(8,128)}, u32[]{:S(2)}) copy-start(f32[24,2048]{1,0:T(8,128)} %copy-done.4) | copy-start | bytes 589828
Sparse Core Ops, SparseCore 0:
  10.3 59.9 all-gather.2
  72.1 55.5 all-gather.4
  631.5 62.6 reduce-scatter.1
